TPU v7x, 32 devices: a whole 2x2x4 slice. The times are simulated.
32 devices in a mesh: kv: 16 (over z, y, x), tp: 2 (over core).
Axes of the slice: x: 2, y: 2, z: 4, core: 2. Of those that a mesh axis runs over, the one named last changes fastest.
Arguments:
- tokens: bfloat16 [128, 2048], P(None, ('kv', 'tp')), may hold values from -16 to 16
- mix_gain: float32 [2048], P('kv'), may hold values from 0.1 to 1.9
- query_weight: bfloat16 [2048, 2048], P('kv', 'tp'), may hold values from -0.125 to 0.125
- key_weight: bfloat16 [2048, 2048], P('kv', 'tp'), may hold values from -0.125 to 0.125
- value_weight: bfloat16 [2048, 2048], P('kv', 'tp'), may hold values from -0.125 to 0.125
- beta_weight: bfloat16 [2048, 16], P('kv', 'tp'), may hold values from -0.125 to 0.125
- decay_weight: bfloat16 [2048, 16], P('kv', 'tp'), may hold values from -0.125 to 0.125
- decay_rate: float32 [16], P('tp'), may hold values from 0.05 to 1
- prior_state: float32 [128, 16, 128, 128], P('kv', 'tp'), may hold values from -1.5 to 1.5
- tail_keys: bfloat16 [128, 16, 64, 128], P('kv', 'tp'), may hold values from -6 to 6
- tail_values: bfloat16 [128, 16, 64, 128], P('kv', 'tp'), may hold values from -6 to 6
- tail_beta: float32 [128, 16, 64], P('kv', 'tp'), may hold values from 0.1 to 0.9
- tail_decay: float32 [128, 16, 64], P('kv', 'tp'), may hold values from -2 to 0
- lengths: int32 [128], P('kv'), may hold values from 1 to 64, 3276 in all
- out_weight: bfloat16 [2048, 2048], P('tp', 'kv'), may hold values from -0.375 to 0.375
- mlp_gain: float32 [2048], P('kv'), may hold values from 0.1 to 1.9
- up_weight: bfloat16 [2048, 8192], P('kv', 'tp'), may hold values from -0.125 to 0.125
- down_weight: bfloat16 [8192, 2048], P('tp', 'kv'), may hold values from -0.0625 to 0.0625
Outputs:
- mixed: bfloat16 [128, 2048], P(None, ('kv', 'tp'))
All inputs are finite; a program needn't handle non-finite values. No bound on the sum of `lengths` on one device may be relied on, other than what follows from the above.
Results may differ from a plain program's by a relative error of at most 0.013.
Values may be sent and summed in bfloat16 or wider, within the bound.
A program may use at most 64 MiB of HBM per device.

v0:
```python
import jax
import jax.numpy as jnp
from jax import lax
from jax.sharding import PartitionSpec as P

D = 2048


epsilon = 1e-06


def unit_rows(vectors):
    return vectors * lax.rsqrt(jnp.sum(vectors * vectors, axis=-1, keepdims=True) + epsilon)


def delta_read(
    previous_state,
    keys,
    value_vectors,
    betas,
    decays,
    live_count,
    queries,
    new_key,
    new_value,
    new_beta,
    new_decay,
):
    peak_value = lax.Precision.HIGHEST
    positions = keys.shape[1]
    head_dim = keys.shape[2]
    live_mask = jnp.arange(positions, dtype=jnp.int32)[None, :] < live_count[:, None]
    unit_keys = unit_rows(keys.astype(jnp.float32))
    value_rows = value_vectors.astype(jnp.float32)
    beta_live = jnp.where(live_mask, betas, 0.0)
    decay_live = jnp.where(live_mask, decays, 0.0)
    cumulative = jnp.cumsum(decay_live, axis=1)
    row_index = jnp.arange(positions, dtype=jnp.int32)
    strict = (row_index[:, None] > row_index[None, :])[None]
    log_gap = cumulative[:, :, None] - cumulative[:, None, :]
    key_intersection = jnp.einsum("nik,njk->nij", unit_keys, unit_keys, precision=peak_value)
    lower_part = jnp.where(
        strict,
        beta_live[:, :, None] * jnp.exp(jnp.where(strict, log_gap, 0.0)) * key_intersection,
        0.0,
    )
    system = lower_part + jnp.eye(positions, dtype=jnp.float32)[None]
    right_sides = jnp.concatenate(
        [
            (beta_live * jnp.exp(cumulative))[:, :, None] * unit_keys,
            beta_live[:, :, None] * value_rows,
        ],
        axis=2,
    )
    solved = jax.scipy.linalg.solve_triangular(system, right_sides, lower=True, unit_diagonal=True)
    weight_matrix_rows = solved[:, :, :head_dim]
    unscaled_rows = solved[:, :, head_dim:]
    adjusted_result = unscaled_rows - jnp.einsum(
        "mfd,mdx->mfx", weight_matrix_rows, previous_state, precision=peak_value
    )
    intersection = jnp.sum(new_key * queries, axis=1)
    test_vector = queries - (new_beta * intersection)[:, None] * new_key
    total_decay = cumulative[:, -1]
    state_readout = jnp.einsum("rq,rqt->rt", test_vector, previous_state, precision=peak_value)
    tail_weights = jnp.exp(total_decay[:, None] - cumulative) * jnp.einsum(
        "njk,nk->nj", unit_keys, test_vector, precision=peak_value
    )
    from_tail = jnp.einsum("nj,njv->nv", tail_weights, adjusted_result, precision=peak_value)
    readout = jnp.exp(total_decay)[:, None] * state_readout + from_tail
    return jnp.exp(new_decay)[:, None] * readout + (new_beta * intersection)[:, None] * new_value


def local(
    tokens,
    mix_gain,
    query_weight,
    key_weight,
    value_weight,
    beta_weight,
    decay_weight,
    decay_rate,
    prior_state,
    tail_keys,
    tail_values,
    tail_beta,
    tail_decay,
    lengths,
    out_weight,
    mlp_gain,
    up_weight,
    down_weight,
):
    own_rows = prior_state.shape[0]
    heads_here = prior_state.shape[1]
    head_dim = prior_state.shape[2]
    tail_span = tail_keys.shape[2]
    token_rows = lax.all_gather(tokens, "tp", axis=1, tiled=True)
    token_float = token_rows.astype(jnp.float32)
    square_part = jnp.sum(token_float * token_float, axis=1)
    normed = (token_float * mix_gain[None, :]).astype(jnp.bfloat16)
    query_part = jnp.dot(normed, query_weight, preferred_element_type=jnp.float32)
    key_part = jnp.dot(normed, key_weight, preferred_element_type=jnp.float32)
    value_part = jnp.dot(normed, value_weight, preferred_element_type=jnp.float32)
    beta_part = jnp.dot(normed, beta_weight, preferred_element_type=jnp.float32)
    decay_part = jnp.dot(normed, decay_weight, preferred_element_type=jnp.float32)
    square_total = lax.psum(square_part, "kv")
    summed = (
        lax.psum_scatter(query_part, "kv", scatter_dimension=0, tiled=True),
        lax.psum_scatter(key_part, "kv", scatter_dimension=0, tiled=True),
        lax.psum_scatter(value_part, "kv", scatter_dimension=0, tiled=True),
        lax.psum_scatter(beta_part, "kv", scatter_dimension=0, tiled=True),
        lax.psum_scatter(decay_part, "kv", scatter_dimension=0, tiled=True),
    )
    own_squares = lax.dynamic_slice_in_dim(square_total, lax.axis_index("kv") * own_rows, own_rows)
    row_scale = lax.rsqrt(own_squares / D + epsilon)[:, None]

    def by_heads(raw):
        return raw.reshape(own_rows, heads_here, head_dim)

    queries = unit_rows(jax.nn.silu(by_heads(summed[0] * row_scale)))
    new_keys = unit_rows(jax.nn.silu(by_heads(summed[1] * row_scale)))
    new_values = jax.nn.silu(by_heads(summed[2] * row_scale))
    new_beta = jax.nn.sigmoid(summed[3] * row_scale)
    new_decay = -decay_rate[None, :] * jax.nn.softplus(summed[4] * row_scale)
    count = own_rows * heads_here
    readout = delta_read(
        prior_state.reshape(count, head_dim, head_dim),
        tail_keys.reshape(count, tail_span, head_dim),
        tail_values.reshape(count, tail_span, head_dim),
        tail_beta.reshape(count, tail_span),
        tail_decay.reshape(count, tail_span),
        jnp.repeat(lengths, heads_here),
        queries.reshape(count, head_dim),
        new_keys.reshape(count, head_dim),
        new_values.reshape(count, head_dim),
        new_beta.reshape(count),
        new_decay.reshape(count),
    )
    head_out = readout.reshape(own_rows, heads_here * head_dim).astype(jnp.bfloat16)
    attended_block = jnp.dot(
        lax.all_gather(head_out, "kv", axis=0, tiled=True),
        out_weight,
        preferred_element_type=jnp.float32,
    )
    attended = lax.psum_scatter(attended_block, "tp", scatter_dimension=1, tiled=True)
    mixed_in = (tokens.astype(jnp.float32) + attended).astype(jnp.bfloat16)
    mixer_rows = lax.all_gather(mixed_in, "tp", axis=1, tiled=True)
    mixer_float = mixer_rows.astype(jnp.float32)
    mixer_square_part = jnp.sum(mixer_float * mixer_float, axis=1)
    mixer_normed = (mixer_float * mlp_gain[None, :]).astype(jnp.bfloat16)
    up_part = jnp.dot(mixer_normed, up_weight, preferred_element_type=jnp.float32)
    up_total, mixer_squares = lax.psum((up_part, mixer_square_part), "kv")
    hidden_raw = up_total * lax.rsqrt(mixer_squares / D + epsilon)[:, None]
    hidden = jnp.square(jnp.maximum(hidden_raw, 0.0)).astype(jnp.bfloat16)
    down_block = jnp.dot(hidden, down_weight, preferred_element_type=jnp.float32)
    down = lax.psum_scatter(
        down_block.astype(jnp.bfloat16), "tp", scatter_dimension=1, tiled=True
    ).astype(jnp.float32)
    return (mixed_in.astype(jnp.float32) + down).astype(jnp.bfloat16)


def solution(mesh):
    in_specs = (
        P(None, ("kv", "tp")),
        P("kv"),
        P("kv", "tp"),
        P("kv", "tp"),
        P("kv", "tp"),
        P("kv", "tp"),
        P("kv", "tp"),
        P("tp"),
        P("kv", "tp", None, None),
        P("kv", "tp", None, None),
        P("kv", "tp", None, None),
        P("kv", "tp", None),
        P("kv", "tp", None),
        P("kv"),
        P("tp", "kv"),
        P("kv"),
        P("kv", "tp"),
        P("tp", "kv"),
    )
    out_specs = P(None, ("kv", "tp"))
    return jax.shard_map(local, mesh=mesh, in_specs=in_specs, out_specs=out_specs, check_vma=False)
```

profile of v0, /device:TPU:0, one launch (start us, length us, event | category | flops | bytes accessed | tf_op | source)
XLA Modules:
  0.0 443.1 jit_solution(13488446043349413590)
XLA Ops:
  6.6 2.3 all_gather.9
  8.9 2.1 fusion.38
  11.1 2.2 fusion.42
  16.6 80.3 %all-reduce.2 = (f32[128]{0:T(128)S(1)}, f32[128,8]{1,0:T(8,128)S(1)}, f32[128,8]{1,0:T(8,128)S(1)}) all-reduce(f32[128]{0:T(128)S(1)} %fusion.10, f32[128,8]{1,0:T(8,128)S(1)} %fusion.40, f32[128,8]{1,0:T(8,128)S(1)} %fusion.44), channel_id=1, replica_groups=mesh['kv'=16,'tp'=2] {'kv'}, use_global_device_ids=true, to_apply=%region_2.0 | all-reduce | flops 2176 | bytes 17408 | tf_op jit(solution)/shard_map/psum | solution.py:106
  98.4 3.3 broadcast_multiply_fusion
  101.7 4.7 %fusion.48 = f32[64,64,64]{2,1,0:T(8,128)} fusion(f32[64,64,128]{2,1,0:T(8,128)S(1)} %get-tuple-element.17), kind=kOutput, calls=%fused_computation.88 | convolution fusion | flops 402653184 | bytes 3145728 | tf_op jit(solution)/shard_map/nik,njk->nij/dot_general | solution.py:41
  106.4 3.4 copy.34
  109.9 6.8 %add_bitcast_fusion = f32[64,1,64,64]{0,3,2,1:T(8,128)} fusion(f32[64,64,64]{0,2,1:T(8,128)} %copy.34, f32[64,64]{1,0:T(8,128)S(1)} %get-tuple-element.27, f32[64,64]{1,0:T(8,128)S(1)} %get-tuple-element.26, f32[64,64]{0,1:T(8,128)S(1)} %copy.32, f32[64,64]{0,1:T(8,128)S(1)} %copy.31, pred[64,64]{1,0:T(8,128)(4,1)S(1)} %get-tuple-element.24, ...), kind=kLoop, calls=%fused_computation.11 | loop fusion | flops 2097152 | bytes 2170880 | tf_op jit(solution)/shard_map/jit(_solve_triangular)/vmap()/triangular_solve | solution.py:55
  116.8 68.4 %custom-call.4 = f32[64,1,64,64]{0,2,3,1:T(8,128)} custom-call(f32[64,1,64,64]{0,3,2,1:T(8,128)} %add_bitcast_fusion), custom_call_target="InvertDiagBlocksLowerTriangular" | custom-call | tf_op jit(solution)/shard_map/jit(_solve_triangular)/vmap()/triangular_solve | solution.py:55
  185.2 4.2 copy.35
  189.3 3.1 convert_multiply_fusion
  192.6 6.9 %fusion = f32[64,64,256]{2,1,0:T(8,128)S(1)} fusion(f32[64,64,64]{2,1,0:T(8,128)} %copy.35, f32[64,64,128]{2,1,0:T(8,128)} %convert_multiply_fusion, f32[64,64,128]{2,1,0:T(8,128)} %get-tuple-element.16), kind=kOutput, calls=%fused_computation | convolution fusion | flops 806354944 | bytes 9437184 | tf_op jit(solution)/shard_map/jit(_solve_triangular)/vmap()/triangular_solve | solution.py:55
  199.4 2.0 copy-done.2
  201.4 5.2 %fusion.4 = f32[64,64,128]{2,1,0:T(8,128)} fusion(f32[64,128,128]{2,1,0:T(8,128)S(1)} %bitcast.80, f32[64,64,256]{2,1,0:T(8,128)S(1)} %fusion), kind=kOutput, calls=%fused_computation.4 | convolution fusion | flops 805306368 | bytes 8388608 | tf_op jit(solution)/shard_map/mfd,mdx->mfx/dot_general | solution.py:58
  208.2 3.3 fusion.47
  211.6 5.6 %fusion.46 = f32[64,1,128]{2,1,0:T(1,128)S(1)} fusion(f32[64,128,1]{1,2,0:T(1,128)S(1)} %bitcast.83, f32[64,128,128]{2,1,0:T(8,128)} %bitcast.79), kind=kOutput, calls=%fused_computation.86 | convolution fusion | flops 12582912 | bytes 4259840 | tf_op jit(solution)/shard_map/rq,rqt->rt/dot_general | solution.py:64
  217.2 26.7 %reduce-scatter.10.cloned.1.call-done = f32[8,1024]{1,0:T(8,128)} async-done(((f32[128,1024]{1,0:T(8,128)}), f32[8,1024]{1,0:T(8,128)}) %reduce-scatter.10.cloned.1.call-update) | async-done | bytes 32784 | tf_op jit(solution)/shard_map/reduce_scatter | solution.py:110
  244.8 3.4 fusion.6
  248.4 37.6 %all_gather.10 = bf16[128,1024]{1,0:T(8,128)(2,1)S(1)} all-gather(bf16[8,1024]{1,0:T(8,128)(2,1)S(1)} %convert_element_type.71), channel_id=1, replica_groups=mesh['kv'=16,'tp'=2] {'kv'}, dimensions={0}, use_global_device_ids=true | all-gather | bytes 278528 | tf_op jit(solution)/shard_map/all_gather | solution.py:141
  286.9 4.8 %reduce-scatter.12.cloned.1.call-done = f32[128,64]{0,1:T(8,128)} async-done(((f32[128,128]{0,1:T(8,128)}), f32[128,64]{0,1:T(8,128)}) %reduce-scatter.12.cloned.1.call-update) | async-done | bytes 32784 | tf_op jit(solution)/shard_map/reduce_scatter | solution.py:145
  296.3 42.7 %psum.23 = f32[128]{0:T(128)S(1)} all-reduce(f32[128]{0:T(128)S(1)} %fusion.12), channel_id=1, replica_groups=mesh['kv'=16,'tp'=2] {'kv'}, use_global_device_ids=true, to_apply=%region_15.16 | all-reduce | flops 128 | bytes 1024 | tf_op jit(solution)/shard_map/psum | solution.py:152
  339.0 86.2 %all-reduce.5.cloned.1.call-done = f32[128,4096]{1,0:T(8,128)} async-done(((f32[128,4096]{1,0:T(8,128)}), f32[128,4096]{1,0:T(8,128)}) %all-reduce.5.cloned.1.call-update) | async-done | bytes 2097168 | tf_op jit(solution)/shard_map/psum | solution.py:152
  425.2 2.8 convolution_convert_fusion
  428.0 6.9 %reduce-scatter.14.cloned.1.call-done = bf16[128,64]{0,1:T(8,128)(2,1)} async-done(((bf16[128,128]{0,1:T(8,128)(2,1)}), bf16[128,64]{0,1:T(8,128)(2,1)}) %reduce-scatter.14.cloned.1.call-update) | async-done | bytes 16400 | tf_op jit(solution)/shard_map/reduce_scatter | solution.py:156
  (95 shorter events, 13.9 us)
Async XLA Ops:
  6.5 287.8 %copy-start = (bf16[128,4096]{1,0:T(8,128)(2,1)S(1)}, bf16[128,4096]{1,0:T(8,128)(2,1)}, u32[]{:S(2)}) copy-start(bf16[128,4096]{1,0:T(8,128)(2,1)} %param.34) | copy-start | bytes 3145732
  6.5 6.8 %copy-start.11 = (f32[128]{0:T(128)S(1)}, f32[128]{0:T(128)}, u32[]{:S(2)}) copy-start(f32[128]{0:T(128)} %param.19) | copy-start | bytes 1540
  6.5 6.8 %copy-start.7 = (bf16[128,1024]{1,0:T(8,128)(2,1)S(1)}, bf16[128,1024]{1,0:T(8,128)(2,1)}, u32[]{:S(2)}) copy-start(bf16[128,1024]{1,0:T(8,128)(2,1)} %param.22) | copy-start | bytes 786436
  6.5 8.1 %copy-start.14 = (s32[8]{0:T(128)S(1)}, s32[8]{0:T(128)}, u32[]{:S(2)}) copy-start(s32[8]{0:T(128)} %param.31) | copy-start | bytes 100
  6.5 8.2 %copy-start.9 = (f32[8,8,64]{2,1,0:T(8,128)S(1)}, f32[8,8,64]{2,1,0:T(8,128)}, u32[]{:S(2)}) copy-start(f32[8,8,64]{2,1,0:T(8,128)} %param.30) | copy-start | bytes 49156
  6.5 200.1 %reduce-scatter.8.cloned.1.call-start = ((), (), s32[]{:S(2)}) async-start(), calls=%async_computation.6 | async-start | bytes 557056 | tf_op jit(solution)/shard_map/reduce_scatter | solution.py:109
  8.9 6.4 %copy-start.12 = (bf16[128,8]{0,1:T(8,128)(2,1)S(1)}, bf16[128,8]{0,1:T(8,128)(2,1)}, u32[]{:S(2)}) copy-start(bf16[128,8]{0,1:T(8,128)(2,1)} %param.23) | copy-start | bytes 6148
  8.9 6.7 %copy-start.13 = (bf16[128,8]{0,1:T(8,128)(2,1)S(1)}, bf16[128,8]{0,1:T(8,128)(2,1)}, u32[]{:S(2)}) copy-start(bf16[128,8]{0,1:T(8,128)(2,1)} %param.24) | copy-start | bytes 6148
  11.0 4.9 %copy-start.10 = (f32[8,8,64]{2,1,0:T(8,128)S(1)}, f32[8,8,64]{2,1,0:T(8,128)}, u32[]{:S(2)}) copy-start(f32[8,8,64]{2,1,0:T(8,128)} %param.29) | copy-start | bytes 49156
  11.0 5.0 %copy-start.4 = (bf16[8,8,64,128]{3,2,1,0:T(8,128)(2,1)S(1)}, bf16[8,8,64,128]{3,2,1,0:T(8,128)(2,1)}, u32[]{:S(2)}) copy-start(bf16[8,8,64,128]{3,2,1,0:T(8,128)(2,1)} %param.27) | copy-start | bytes 3145732
  11.0 5.6 %copy-start.16 = (f32[8]{0:T(128)S(1)}, f32[8]{0:T(128)}, u32[]{:S(2)}) copy-start(f32[8]{0:T(128)} %param.25) | copy-start | bytes 100
  11.1 195.6 %reduce-scatter.6.cloned.1.call-start = ((), (), s32[]{:S(2)}) async-start(), calls=%async_computation.5 | async-start | bytes 557056 | tf_op jit(solution)/shard_map/reduce_scatter | solution.py:108
  13.3 83.7 %copy-start.17 = (u32[32]{0:T(128)S(1)}, u32[32]{0:T(128)}, u32[]{:S(2)}) copy-start(u32[32]{0:T(128)} %constant.51) | copy-start | bytes 388
  13.3 230.6 %reduce-scatter.10.cloned.1.call-start = ((), (), s32[]{:S(2)}) async-start(), calls=%async_computation.7 | async-start | bytes 557056 | tf_op jit(solution)/shard_map/reduce_scatter | solution.py:110
  14.5 277.2 %reduce-scatter.12.cloned.1.call-start = ((), (), s32[]{:S(2)}) async-start(), calls=%async_computation.8 | async-start | bytes 98304 | tf_op jit(solution)/shard_map/reduce_scatter | solution.py:145
  192.6 8.9 %copy-start.1 = (f32[8,8,128,128]{3,2,1,0:T(8,128)S(1)}, f32[8,8,128,128]{3,2,1,0:T(8,128)}, u32[]{:S(2)}) copy-start(f32[8,8,128,128]{3,2,1,0:T(8,128)} %param.26) | copy-start | bytes 12582916
  199.4 2.0 copy-start.2
  211.6 33.2 %copy-start.3 = (f32[64,64,128]{2,1,0:T(8,128)S(1)}, f32[64,64,128]{2,1,0:T(8,128)}, u32[]{:S(2)}) copy-start(f32[64,64,128]{2,1,0:T(8,128)} %fusion.4) | copy-start | bytes 6291460
  244.8 41.1 %copy-start.6 = (bf16[1024,128]{1,0:T(8,128)(2,1)S(1)}, bf16[1024,128]{1,0:T(8,128)(2,1)}, u32[]{:S(2)}) copy-start(bf16[1024,128]{1,0:T(8,128)(2,1)} %param.32) | copy-start | bytes 786436
  244.8 46.9 %copy-start.8 = (bf16[128,64]{0,1:T(8,128)(2,1)S(1)}, bf16[128,64]{0,1:T(8,128)(2,1)}, u32[]{:S(2)}) copy-start(bf16[128,64]{0,1:T(8,128)(2,1)} %param.18) | copy-start | bytes 49156
  244.8 49.5 %copy-start.15 = (f32[128]{0:T(128)S(1)}, f32[128]{0:T(128)}, u32[]{:S(2)}) copy-start(f32[128]{0:T(128)} %param.33) | copy-start | bytes 1540
  286.9 138.3 %all-reduce.5.cloned.1.call-start = ((), (), s32[]{:S(2)}) async-start(), calls=%async_computation.9 | async-start | bytes 4194304 | tf_op jit(solution)/shard_map/psum | solution.py:152
  294.3 130.9 %copy-start.5 = (bf16[4096,128]{1,0:T(8,128)(2,1)S(1)}, bf16[4096,128]{1,0:T(8,128)(2,1)}, u32[]{:S(2)}) copy-start(bf16[4096,128]{1,0:T(8,128)(2,1)} %param.35) | copy-start | bytes 3145732
  296.2 138.8 %reduce-scatter.14.cloned.1.call-start = ((), (), s32[]{:S(2)}) async-start(), calls=%async_computation.10 | async-start | bytes 49152 | tf_op jit(solution)/shard_map/reduce_scatter | solution.py:156
Sparse Core Ops, SparseCore 0:
  11.2 80.3 reduce-scatter.7
  93.8 73.8 reduce-scatter.5
  169.9 73.8 reduce-scatter.9
  287.0 4.6 reduce-scatter.11
  297.0 128.0 all-reduce.4
  428.2 6.7 reduce-scatter.13
where the time goes:
time: 444 us; the launch traced here: 443 us
  blocking collectives  165 us (37%)
  waiting for transfers between devices  125 us (28%)
  other arithmetic  87.4 us (20%)
  matrix products  40.5 us (9%)
  between operations  14.4 us (3%)
  local copies, waits for them, and re-layouts  11.2 us (3%)
    psum x1, waiting for transfers between devices, local(): up_total, mixer_squares = lax.psum((up_part, mixer_square_part), 'kv')  86.2 us
    psum x1, blocking collectives, local(): square_total = lax.psum(square_part, 'kv')  80.3 us
    another operation x3, other arithmetic, delta_read(): jax.scipy.linalg.solve_triangular(system, right_sides, lower=True, unit_d...  75.3 us
    psum x1, blocking collectives, local(): up_total, mixer_squares = lax.psum((up_part, mixer_square_part), 'kv')  42.7 us
    all_gather x1, blocking collectives, local(): lax.all_gather(head_out, 'kv', axis=0, tiled=True)  37.6 us
    reduce_scatter x1, waiting for transfers between devices, local(): lax.psum_scatter(value_part, 'kv', scatter_dimension=0, tiled=True)  26.7 us
  transfers between devices with their start and end apart: 6, of which 4 were waited for; matrix products, arithmetic and copies ran while one was open for 28% of the time, Pallas kernels for 0%

commit v1 on v0

v1 whole, which is shorter than its diff:
```python
import functools

import jax
import jax.numpy as jnp
from jax import lax
from jax.experimental import pallas as pl
from jax.experimental.pallas import tpu as pltpu
from jax.sharding import PartitionSpec as P

epsilon = 1e-06
LINK = jnp.bfloat16
F32 = jnp.float32
MESH = pl.DeviceIdType.MESH


def peer_of(axis, offset, count):
    return lax.rem(lax.axis_index(axis) + offset, count)


def greet(groups):
    barrier = pltpu.get_barrier_semaphore()
    for axis, count in groups:
        for offset in range(1, count):
            pl.semaphore_signal(
                barrier, inc=1, device_id={axis: peer_of(axis, offset, count)}, device_id_type=MESH
            )


def greeted(groups):
    barrier = pltpu.get_barrier_semaphore()
    pl.semaphore_wait(barrier, sum(count - 1 for _, count in groups))


def send(src, dst, send_sem, recv_sem, axis, peer):
    copy = pltpu.make_async_remote_copy(
        src_ref=src,
        dst_ref=dst,
        send_sem=send_sem,
        recv_sem=recv_sem,
        device_id={axis: peer},
        device_id_type=MESH,
    )
    copy.start()
    return copy


def exchange_rows(parts, arrivals, send_sems, recv_sems, count):
    copies = []
    for offset in range(1, count):
        peer = peer_of("kv", offset, count)
        copies.append(
            send(parts.at[peer], arrivals.at[offset], send_sems.at[offset], recv_sems.at[offset], "kv", peer)
        )
    return copies


def gathered_sum(parts, arrivals, copies, count):
    total = parts[lax.axis_index("kv")].astype(F32)
    for offset in range(1, count):
        copies[offset - 1].wait_recv()
        total = total + arrivals[offset].astype(F32)
    return total


def split_rows(block, count):
    return block.reshape(count, block.shape[0] // count, block.shape[1])


def project_kernel(
    count,
    heads,
    tokens,
    gain,
    query_w,
    key_w,
    value_w,
    small_w,
    query_o,
    key_o,
    value_o,
    small_o,
    small_parts,
    small_in,
    parts,
    arrivals,
    send_sems,
    recv_sems,
):
    groups = (("kv", count),)
    greet(groups)
    token_float = tokens[...].astype(F32)
    normed = (token_float * gain[...]).astype(jnp.bfloat16)
    small = jnp.dot(normed, small_w[...], preferred_element_type=F32)
    squares = jnp.sum(token_float * token_float, axis=1, keepdims=True)
    lane = lax.broadcasted_iota(jnp.int32, small.shape, 1)
    small_parts[...] = split_rows(jnp.where(lane == 2 * heads, squares, small), count)
    greeted(groups)
    flights = [exchange_rows(small_parts, small_in, send_sems.at[3], recv_sems.at[3], count)]
    for index, weight in enumerate((query_w, key_w, value_w)):
        block = jnp.dot(normed, weight[...], preferred_element_type=F32)
        parts[index] = split_rows(block, count).astype(LINK)
        flights.append(
            exchange_rows(parts.at[index], arrivals.at[index], send_sems.at[index], recv_sems.at[index], count)
        )
    small_o[...] = gathered_sum(small_parts, small_in, flights[0], count)
    for index, out in enumerate((query_o, key_o, value_o)):
        out[...] = gathered_sum(parts.at[index], arrivals.at[index], flights[index + 1], count)
    for flight in flights:
        for copy in flight:
            copy.wait_send()


def unit_rows(vectors):
    return vectors * lax.rsqrt(jnp.sum(vectors * vectors, axis=-1, keepdims=True) + epsilon)


def silu(x):
    return x * jax.nn.sigmoid(x)


def softplus(x):
    return jnp.maximum(x, 0.0) + jnp.log(1.0 + jnp.exp(-jnp.abs(x)))


def delta_kernel(
    width,
    query_r,
    key_r,
    value_r,
    small_r,
    rate,
    lengths,
    betas,
    decays,
    keys,
    values,
    state,
    out,
    keys32,
    values32,
    rows_scr,
):
    rows, heads, head_dim = state.shape[0], state.shape[1], state.shape[2]
    span = betas.shape[2]

    def stack(pieces):
        return jnp.concatenate(pieces, axis=0)

    keys32[...] = keys[...].astype(F32)
    values32[...] = values[...].astype(F32)
    small = small_r[...]
    scale = lax.rsqrt(small[:, 2 * heads : 2 * heads + 1] / width + epsilon)
    scaled = small * scale

    def by_heads(ref):
        raw = ref[...] * scale
        return stack([raw[:, h * head_dim : (h + 1) * head_dim] for h in range(heads)])

    queries = unit_rows(silu(by_heads(query_r)))
    new_key = unit_rows(silu(by_heads(key_r)))
    new_value = silu(by_heads(value_r))
    new_beta = stack([jax.nn.sigmoid(scaled[:, h : h + 1]) for h in range(heads)])
    new_decay = stack(
        [-rate[0, h] * softplus(scaled[:, heads + h : heads + h + 1]) for h in range(heads)]
    )
    live = lax.broadcasted_iota(jnp.int32, (rows, span), 1) < lengths[...]
    beta_live = stack([jnp.where(live, betas[:, h, :], 0.0) for h in range(heads)])
    shrink = stack([jnp.exp(jnp.where(live, decays[:, h, :], 0.0)) for h in range(heads)])

    meet = new_beta * jnp.sum(new_key * queries, axis=1, keepdims=True)
    fade = jnp.exp(new_decay)
    probe = (queries - meet * new_key) * fade
    read = meet * new_value
    for t in range(span - 1, -1, -1):
        k = stack([keys32[pl.ds(h * span + t, rows, stride=heads * span), :] for h in range(heads)])
        v = stack([values32[pl.ds(h * span + t, rows, stride=heads * span), :] for h in range(heads)])
        inverse = lax.rsqrt(jnp.sum(k * k, axis=1, keepdims=True) + epsilon)
        unit = k * inverse
        hit = beta_live[:, t : t + 1] * jnp.sum(unit * probe, axis=1, keepdims=True)
        read = read + hit * v
        probe = shrink[:, t : t + 1] * (probe - hit * unit)
    total = rows * heads
    if total < head_dim:
        probe = jnp.concatenate([probe, jnp.zeros((head_dim - total, head_dim), F32)], axis=0)
    columns = probe.T
    for h in range(heads):
        for r in range(rows):
            n = h * rows + r
            rows_scr[n : n + 1, :] = jnp.sum(columns[:, n : n + 1] * state[r, h], axis=0, keepdims=True)
    final = read + rows_scr[...]
    for h in range(heads):
        out[:, h * head_dim : (h + 1) * head_dim] = final[h * rows : (h + 1) * rows].astype(jnp.bfloat16)


def across_heads(block, mine, arrivals, send_sems, recv_sems, count):
    mine[...] = block
    copies = []
    for offset in range(1, count):
        peer = peer_of("tp", offset, count)
        copies.append(send(mine, arrivals.at[offset], send_sems.at[offset], recv_sems.at[offset], "tp", peer))
    total = block
    for offset in range(1, count):
        copies[offset - 1].wait_recv()
        total = total + arrivals[offset]
    return total, copies


def spread(own, everywhere, send_sems, recv_sems, count):
    me = lax.axis_index("kv")
    return [
        send(own, everywhere.at[me], send_sems.at[offset], recv_sems.at[offset], "kv", peer_of("kv", offset, count))
        for offset in range(1, count)
    ]


def whole_rows(everywhere, dtype):
    block = everywhere[...].astype(F32)
    return block.reshape(block.shape[0] * block.shape[1], block.shape[2]).astype(dtype)


def mixer_kernel(
    count,
    tp_count,
    width,
    head_out,
    tokens,
    gain,
    out_w,
    up_w,
    down_w,
    result,
    heads_all,
    share,
    share_in,
    down_share,
    down_in,
    square_parts,
    square_in,
    parts,
    arrivals,
    hidden_own,
    hidden_all,
    kv_send,
    kv_recv,
    tp_send,
    tp_recv,
):
    groups = (("kv", count), ("tp", tp_count))
    pieces, piece = parts.shape[0], parts.shape[3]
    me = lax.axis_index("kv")
    greet(groups)
    heads_all[me] = head_out[...]
    greeted(groups)
    flights = [spread(head_out, heads_all, kv_send.at[0], kv_recv.at[0], count)]
    for copy in flights[0]:
        copy.wait_recv()
    attended = jnp.dot(whole_rows(heads_all, jnp.bfloat16), out_w[...], preferred_element_type=F32)
    attended, copies = across_heads(attended, share, share_in, tp_send.at[0], tp_recv.at[0], tp_count)
    flights.append(copies)
    mixed_in = (tokens[...].astype(F32) + attended).astype(jnp.bfloat16).astype(F32)
    squares = jnp.sum(mixed_in * mixed_in, axis=1, keepdims=True)
    square_parts[...] = split_rows(jnp.broadcast_to(squares, (squares.shape[0], 128)), count)
    square_flight = exchange_rows(square_parts, square_in, kv_send.at[1], kv_recv.at[1], count)
    normed = (mixed_in * gain[...]).astype(jnp.bfloat16)
    up_flights = []
    for p in range(pieces):
        block = jnp.dot(normed, up_w[:, p * piece : (p + 1) * piece], preferred_element_type=F32)
        parts[p] = split_rows(block, count).astype(LINK)
        up_flights.append(
            exchange_rows(parts.at[p], arrivals.at[p], kv_send.at[2 + p], kv_recv.at[2 + p], count)
        )
    own_squares = gathered_sum(square_parts, square_in, square_flight, count)
    scale = lax.rsqrt(own_squares[:, :1] / width + epsilon)
    down_flights = []
    for p in range(pieces):
        raw = gathered_sum(parts.at[p], arrivals.at[p], up_flights[p], count) * scale
        hidden = jnp.square(jnp.maximum(raw, 0.0)).astype(jnp.bfloat16)
        hidden_own[p] = hidden
        slot = 2 + pieces + p
        down_flights.append(
            spread(hidden_own.at[p], hidden_all.at[p], kv_send.at[slot], kv_recv.at[slot], count)
        )
        hidden_all[p, me] = hidden
    down = jnp.zeros(share.shape, F32)
    for p in range(pieces):
        for copy in down_flights[p]:
            copy.wait_recv()
        down = down + jnp.dot(
            whole_rows(hidden_all.at[p], jnp.bfloat16),
            down_w[p * piece : (p + 1) * piece, :],
            preferred_element_type=F32,
        )
    down, copies = across_heads(down, down_share, down_in, tp_send.at[1], tp_recv.at[1], tp_count)
    flights.append(copies)
    result[...] = (mixed_in + down).astype(jnp.bfloat16)
    for flight in flights + [square_flight] + up_flights + down_flights:
        for copy in flight:
            copy.wait_send()


def vmem(count):
    return [pl.BlockSpec(memory_space=pltpu.VMEM)] * count


def local(
    kv,
    tp,
    tokens,
    mix_gain,
    query_weight,
    key_weight,
    value_weight,
    beta_weight,
    decay_weight,
    decay_rate,
    prior_state,
    tail_keys,
    tail_values,
    tail_beta,
    tail_decay,
    lengths,
    out_weight,
    mlp_gain,
    up_weight,
    down_weight,
):
    rows, heads, head_dim = prior_state.shape[:3]
    span = tail_keys.shape[2]
    batch = rows * kv
    depth = mix_gain.shape[0]
    width = depth * kv
    inner = heads * head_dim
    units = up_weight.shape[1]
    piece = min(units, 1024)
    pieces = units // piece
    dma = pltpu.SemaphoreType.DMA
    token_rows = lax.all_gather(tokens, "tp", axis=1, tiled=True)
    small_weight = jnp.concatenate(
        [beta_weight, decay_weight, jnp.zeros((depth, 128 - 2 * heads), jnp.bfloat16)], axis=1
    )
    query_s, key_s, value_s, small_s = pl.pallas_call(
        functools.partial(project_kernel, kv, heads),
        out_shape=[jax.ShapeDtypeStruct((rows, inner), F32)] * 3 + [jax.ShapeDtypeStruct((rows, 128), F32)],
        in_specs=vmem(6),
        out_specs=vmem(4),
        scratch_shapes=[
            pltpu.VMEM((kv, rows, 128), F32),
            pltpu.VMEM((kv, rows, 128), F32),
            pltpu.VMEM((3, kv, rows, inner), LINK),
            pltpu.VMEM((3, kv, rows, inner), LINK),
            dma((4, kv)),
            dma((4, kv)),
        ],
        compiler_params=pltpu.CompilerParams(
            collective_id=0, has_side_effects=True, vmem_limit_bytes=16 * 2**20
        ),
        name="project",
    )(token_rows, mix_gain.reshape(1, depth), query_weight, key_weight, value_weight, small_weight)
    count = rows * heads * span
    head_out = pl.pallas_call(
        functools.partial(delta_kernel, width),
        out_shape=jax.ShapeDtypeStruct((rows, inner), jnp.bfloat16),
        in_specs=vmem(4) + [pl.BlockSpec(memory_space=pltpu.SMEM)] + vmem(6),
        out_specs=vmem(1)[0],
        scratch_shapes=[
            pltpu.VMEM((count, head_dim), F32),
            pltpu.VMEM((count, head_dim), F32),
            pltpu.VMEM((rows * heads, head_dim), F32),
        ],
        compiler_params=pltpu.CompilerParams(vmem_limit_bytes=32 * 2**20),
        name="delta",
    )(
        query_s,
        key_s,
        value_s,
        small_s,
        decay_rate.reshape(1, heads),
        lengths.reshape(rows, 1),
        tail_beta,
        tail_decay,
        tail_keys.reshape(count, head_dim),
        tail_values.reshape(count, head_dim),
        prior_state,
    )
    slots = 2 + 2 * pieces
    result = pl.pallas_call(
        functools.partial(mixer_kernel, kv, tp, width),
        out_shape=jax.ShapeDtypeStruct((batch, depth), jnp.bfloat16),
        in_specs=vmem(6),
        out_specs=vmem(1)[0],
        scratch_shapes=[
            pltpu.VMEM((kv, rows, inner), jnp.bfloat16),
            pltpu.VMEM((batch, depth), F32),
            pltpu.VMEM((tp, batch, depth), F32),
            pltpu.VMEM((batch, depth), F32),
            pltpu.VMEM((tp, batch, depth), F32),
            pltpu.VMEM((kv, rows, 128), F32),
            pltpu.VMEM((kv, rows, 128), F32),
            pltpu.VMEM((pieces, kv, rows, piece), LINK),
            pltpu.VMEM((pieces, kv, rows, piece), LINK),
            pltpu.VMEM((pieces, rows, piece), jnp.bfloat16),
            pltpu.VMEM((pieces, kv, rows, piece), jnp.bfloat16),
            dma((slots, kv)),
            dma((slots, kv)),
            dma((2, tp)),
            dma((2, tp)),
        ],
        compiler_params=pltpu.CompilerParams(
            collective_id=1, has_side_effects=True, vmem_limit_bytes=32 * 2**20
        ),
        name="mixer",
    )(head_out, token_rows, mlp_gain.reshape(1, depth), out_weight, up_weight, down_weight)
    columns = depth // tp
    return lax.dynamic_slice_in_dim(result, lax.axis_index("tp") * columns, columns, axis=1)


def solution(mesh):
    in_specs = (
        P(None, ("kv", "tp")),
        P("kv"),
        P("kv", "tp"),
        P("kv", "tp"),
        P("kv", "tp"),
        P("kv", "tp"),
        P("kv", "tp"),
        P("tp"),
        P("kv", "tp", None, None),
        P("kv", "tp", None, None),
        P("kv", "tp", None, None),
        P("kv", "tp", None),
        P("kv", "tp", None),
        P("kv"),
        P("tp", "kv"),
        P("kv"),
        P("kv", "tp"),
        P("tp", "kv"),
    )
    out_specs = P(None, ("kv", "tp"))
    body = functools.partial(local, mesh.shape["kv"], mesh.shape["tp"])
    return jax.shard_map(body, mesh=mesh, in_specs=in_specs, out_specs=out_specs, check_vma=False)
```

time: 444 us -> 120 us (0.27)
  blocking collectives: 165 us -> 2.3 us
  waiting for transfers between devices: 125 us -> 0 us
  Pallas kernels: 0 us -> 104 us
  other arithmetic: 87.4 us -> 0.09 us
  matrix products: 40.5 us -> 0 us
  between operations: 14.4 us -> 0.09 us
    psum x2 -> x0, blocking collectives: 123 us -> none  [the longest x1 80.3 us: local(): square_total = lax.psum(square_part, 'kv')]
    pallas_call x0 -> x3, Pallas kernels: none -> 104 us  [the longest x1 64.7 us: local(): pl.pallas_call(functools.partial(mixer_kernel, kv, tp, width), out_shape=...]
    psum x1 -> x0, waiting for transfers between devices: 86.2 us -> none  [local(): up_total, mixer_squares = lax.psum((up_part, mixer_square_part), 'kv')]
    another operation x4 -> x0, other arithmetic: 75.5 us -> none  [the longest x3 75.3 us: delta_read(): jax.scipy.linalg.solve_triangular(system, right_sides, lower=True, unit_d...]
    all_gather x2 -> x0, blocking collectives: 39.4 us -> none  [the longest x1 37.6 us: local(): lax.all_gather(head_out, 'kv', axis=0, tiled=True)]
    reduce_scatter x5 -> x0, waiting for transfers between devices: 38.4 us -> none  [the longest x1 26.7 us: local(): lax.psum_scatter(value_part, 'kv', scatter_dimension=0, tiled=True)]
    dot_general x13 -> x0, matrix products: 33.6 us -> none  [the longest x1 5.6 us: delta_read(): jnp.einsum('rq,rqt->rt', test_vector, previous_state, precision=peak_value)]
    unnamed x37 -> x30, local copies, waits for them, and re-layouts: 2.67 us -> 11.9 us
  transfers between devices with their start and end apart: 6 -> 0, of which waited for: 4 -> 0; matrix products, arithmetic and copies ran while one was open for 28% -> 0% of each run, Pallas kernels for 0% -> 0%
where the time goes in v1:
time: 120 us
  Pallas kernels  104 us (87%)
  local copies, waits for them, and re-layouts  13.6 us (11%)
  blocking collectives  2.3 us (2%)
    pallas_call x1, Pallas kernels, local(): pl.pallas_call(functools.partial(mixer_kernel, kv, tp, width), out_shape=...  64.7 us
    pallas_call x1, Pallas kernels, local(): pl.pallas_call(functools.partial(project_kernel, kv, heads), out_shape=[j...  25.4 us
    pallas_call x1, Pallas kernels, local(): pl.pallas_call(functools.partial(delta_kernel, width), out_shape=jax.Shap...  13.8 us
    unnamed x30, local copies, waits for them, and re-layouts  11.9 us

profile of v1, /device:TPU:0, one launch (start us, length us, event | category | flops | bytes accessed | tf_op | source)
XLA Modules:
  0.0 119.9 jit_solution(3620824621967820106)
XLA Ops:
  0.0 2.3 %all_gather.3 = bf16[128,128]{0,1:T(8,128)(2,1)S(1)} all-gather(bf16[128,64]{0,1:T(8,128)(2,1)} %param.18), channel_id=1, replica_groups=mesh['kv'=16,'tp'=2] {'tp'}, dimensions={1}, use_global_device_ids=true | all-gather | bytes 49152 | tf_op jit(solution)/shard_map/all_gather | solution.py:337
  2.3 0.1 copy.26.tokens
  2.4 0.8 copy.24
  3.2 0.8 copy.25
  4.0 0.1 pad.2.clone
  4.1 0.1 maximum_maximum_fusion.small_w
  4.2 0.0 copy-start.5
  4.2 0.9 copy-done.5
  5.2 0.9 copy-done.6
  6.1 0.9 copy-done.7
  7.1 0.7 copy-done.11
  7.7 25.4 %project.1 = (f32[8,1024]{1,0:T(8,128)S(1)}, f32[8,1024]{1,0:T(8,128)S(1)}, f32[8,1024]{1,0:T(8,128)S(1)}, f32[8,128]{1,0:T(8,128)S(1)}) custom-call(bf16[128,128]{1,0:T(8,128)(2,1)S(1)} %copy.26.tokens, f32[1,128]{1,0:T(1,128)S(1)} %bitcast.8, bf16[128,1024]{1,0:T(8,128)(2,1)S(1)} %copy-done.5, bf16[128,1024]{1,0:T(8,128)(2,1)S(1)} %copy-done.6, ...), custom_call_target="tpu_custom_call" | custom-call | tf_op jit(solution)/shard_map/project/pallas_call | solution.py:341
  33.1 0.7 copy.27.lengths
  33.9 2.2 %copy-done = f32[8,8,128,128]{3,2,1,0:T(8,128)S(1)} copy-done((f32[8,8,128,128]{3,2,1,0:T(8,128)S(1)}, f32[8,8,128,128]{3,2,1,0:T(8,128)}, u32[]{:S(2)}) %copy-start) | copy-done | bytes 4194328
  36.0 1.2 %copy-done.1 = bf16[8,8,64,128]{3,2,1,0:T(8,128)(2,1)S(1)} copy-done((bf16[8,8,64,128]{3,2,1,0:T(8,128)(2,1)S(1)}, bf16[8,8,64,128]{3,2,1,0:T(8,128)(2,1)}, u32[]{:S(2)}) %copy-start.1) | copy-done | bytes 1048600
  37.3 1.2 %copy-done.2 = bf16[8,8,64,128]{3,2,1,0:T(8,128)(2,1)S(1)} copy-done((bf16[8,8,64,128]{3,2,1,0:T(8,128)(2,1)S(1)}, bf16[8,8,64,128]{3,2,1,0:T(8,128)(2,1)}, u32[]{:S(2)}) %copy-start.2) | copy-done | bytes 1048600
  38.5 0.8 copy-done.9
  39.2 0.8 copy-done.10
  40.0 0.7 copy-done.12
  40.7 13.8 %delta.1.head_out = bf16[8,1024]{1,0:T(8,128)(2,1)S(1)} custom-call(f32[8,1024]{1,0:T(8,128)S(1)} %get-tuple-element.9.query_r, f32[8,1024]{1,0:T(8,128)S(1)} %get-tuple-element.10.key_r, f32[8,1024]{1,0:T(8,128)S(1)} %get-tuple-element.11.value_r, f32[8,128]{1,0:T(8,128)S(1)} %get-tuple-element.12.small_r, f32[1,8]{1,0:T(1,128)S(1)} %bitcast.9, ...), custom_call_target="tpu_custom_call" | custom-call | tf_op jit(solution)/shard_map/delta/pallas_call | solution.py:360
  54.4 0.0 copy-done.3
  54.5 64.7 %mixer.1 = bf16[128,128]{1,0:T(8,128)(2,1)S(1)} custom-call(bf16[8,1024]{1,0:T(8,128)(2,1)S(1)} %delta.1.head_out, bf16[128,128]{1,0:T(8,128)(2,1)S(1)} %copy.26.tokens, f32[1,128]{1,0:T(1,128)S(1)} %bitcast.10, bf16[1024,128]{1,0:T(8,128)(2,1)S(1)} %copy-done.8, bf16[128,4096]{1,0:T(8,128)(2,1)S(1)} %copy-done.3, bf16[4096,128]{1,0:T(8,128)(2,1)S(1)} %copy-done.4), custom_call_target="tpu_custom_call" | custom-call | tf_op jit(solution)/shard_map/mixer/pallas_call | solution.py:386
  119.1 0.1 constant_dynamic-slice_fusion
  119.2 0.7 copy.29
  (17 shorter events, 0.0 us)
Async XLA Ops:
  0.0 54.4 %copy-start.3 = (bf16[128,4096]{1,0:T(8,128)(2,1)S(1)}, bf16[128,4096]{1,0:T(8,128)(2,1)}, u32[]{:S(2)}) copy-start(bf16[128,4096]{1,0:T(8,128)(2,1)} %up_w.1) | copy-start | bytes 3145732
  4.2 1.0 copy-start.5
  5.2 0.9 copy-start.6
  6.1 0.9 copy-start.7
  7.1 0.7 copy-start.11
  7.7 46.7 %copy-start.13 = (f32[128]{0:T(128)S(1)}, f32[128]{0:T(128)}, u32[]{:S(2)}) copy-start(f32[128]{0:T(128)} %param.33) | copy-start | bytes 1540
  33.8 2.2 %copy-start = (f32[8,8,128,128]{3,2,1,0:T(8,128)S(1)}, f32[8,8,128,128]{3,2,1,0:T(8,128)}, u32[]{:S(2)}) copy-start(f32[8,8,128,128]{3,2,1,0:T(8,128)} %state.1) | copy-start | bytes 12582916
  36.0 1.2 %copy-start.1 = (bf16[8,8,64,128]{3,2,1,0:T(8,128)(2,1)S(1)}, bf16[8,8,64,128]{3,2,1,0:T(8,128)(2,1)}, u32[]{:S(2)}) copy-start(bf16[8,8,64,128]{3,2,1,0:T(8,128)(2,1)} %param.27) | copy-start | bytes 3145732
  37.3 1.2 %copy-start.2 = (bf16[8,8,64,128]{3,2,1,0:T(8,128)(2,1)S(1)}, bf16[8,8,64,128]{3,2,1,0:T(8,128)(2,1)}, u32[]{:S(2)}) copy-start(bf16[8,8,64,128]{3,2,1,0:T(8,128)(2,1)} %param.28) | copy-start | bytes 3145732
  38.5 0.8 copy-start.9
  39.2 0.8 copy-start.10
  40.0 0.7 copy-start.12
  40.7 13.8 %copy-start.4 = (bf16[4096,128]{1,0:T(8,128)(2,1)S(1)}, bf16[4096,128]{1,0:T(8,128)(2,1)}, u32[]{:S(2)}) copy-start(bf16[4096,128]{1,0:T(8,128)(2,1)} %down_w.1) | copy-start | bytes 3145732
  40.7 13.8 %copy-start.8 = (bf16[1024,128]{1,0:T(8,128)(2,1)S(1)}, bf16[1024,128]{1,0:T(8,128)(2,1)}, u32[]{:S(2)}) copy-start(bf16[1024,128]{1,0:T(8,128)(2,1)} %out_w.1) | copy-start | bytes 786436

commit v2 on v1

v2 whole, which is shorter than its diff:
```python
import functools
import math

import jax
import jax.numpy as jnp
from jax import lax
from jax.experimental import pallas as pl
from jax.experimental.pallas import tpu as pltpu
from jax.sharding import PartitionSpec as P

epsilon = 1e-06
LINK = jnp.bfloat16
F32 = jnp.float32
MESH = pl.DeviceIdType.MESH


def peer_of(axis, offset, count):
    return lax.rem(lax.axis_index(axis) + offset, count)


def greet(count, tp_count):
    barrier = pltpu.get_barrier_semaphore()
    group = group_of(count)
    met = [{"kv": inner_peer(offset, count)} for offset in range(1, group)]
    met += [{"kv": outer_peer(offset, count)} for offset in range(1, count // group)]
    met += [{"tp": peer_of("tp", offset, tp_count)} for offset in range(1, tp_count)]
    for peer in met:
        pl.semaphore_signal(barrier, inc=1, device_id=peer, device_id_type=MESH)
    return len(met)


def greeted(met):
    pl.semaphore_wait(pltpu.get_barrier_semaphore(), met)


def send(src, dst, send_sem, recv_sem, axis, peer):
    copy = pltpu.make_async_remote_copy(
        src_ref=src,
        dst_ref=dst,
        send_sem=send_sem,
        recv_sem=recv_sem,
        device_id={axis: peer},
        device_id_type=MESH,
    )
    copy.start()
    return copy


def group_of(count):
    return max(size for size in range(1, math.isqrt(count) + 1) if count % size == 0)


def place(count):
    group = group_of(count)
    me = lax.axis_index("kv")
    return me // group, lax.rem(me, group)


def inner_peer(offset, count):
    outer, inner = place(count)
    group = group_of(count)
    return outer * group + lax.rem(inner + offset, group)


def outer_peer(offset, count):
    outer, inner = place(count)
    group = group_of(count)
    return lax.rem(outer + offset, count // group) * group + inner


def put_rows(parts, block, count):
    group = group_of(count)
    rows = block.shape[0] // count
    split = block.reshape(count // group, group, rows, block.shape[1])
    for inner in range(group):
        parts[inner] = split[:, inner].astype(parts.dtype)


def scatter_inner(parts, arrivals, send_sems, recv_sems, count):
    group = group_of(count)
    _, inner = place(count)
    return [
        send(
            parts.at[lax.rem(inner + offset, group)],
            arrivals.at[offset],
            send_sems.at[offset],
            recv_sems.at[offset],
            "kv",
            inner_peer(offset, count),
        )
        for offset in range(1, group)
    ]


def scatter_outer(parts, arrivals, middle, middle_in, copies, send_sems, recv_sems, count):
    group = group_of(count)
    outer, inner = place(count)
    total = parts[inner].astype(F32)
    for offset in range(1, group):
        copies[offset - 1].wait_recv()
        total = total + arrivals[offset].astype(F32)
    middle[...] = total.astype(middle.dtype)
    return [
        send(
            middle.at[lax.rem(outer + offset, count // group)],
            middle_in.at[offset],
            send_sems.at[offset],
            recv_sems.at[offset],
            "kv",
            outer_peer(offset, count),
        )
        for offset in range(1, count // group)
    ]


def gathered_sum(middle, middle_in, copies, count):
    outer, _ = place(count)
    total = middle[outer].astype(F32)
    for offset, copy in enumerate(copies, 1):
        copy.wait_recv()
        total = total + middle_in[offset].astype(F32)
    return total


def gather_outer(everywhere, send_sems, recv_sems, count):
    outer, inner = place(count)
    block = everywhere.at[inner, outer]
    return [
        send(block, block, send_sems.at[offset], recv_sems.at[offset], "kv", outer_peer(offset, count))
        for offset in range(1, count // group_of(count))
    ]


def gather_inner(everywhere, copies, send_sems, recv_sems, count):
    _, inner = place(count)
    for copy in copies:
        copy.wait_recv()
    block = everywhere.at[inner]
    return [
        send(block, block, send_sems.at[offset], recv_sems.at[offset], "kv", inner_peer(offset, count))
        for offset in range(1, group_of(count))
    ]


def all_rows(everywhere):
    block = everywhere[...].astype(F32)
    group, outer, rows, width = block.shape
    return block.reshape(group * outer * rows, width).astype(jnp.bfloat16)


def in_order(block, count):
    group = group_of(count)
    outer = count // group
    split = block.reshape(group, outer, block.shape[0] // count, block.shape[1])
    return jnp.concatenate([split[i, o] for o in range(outer) for i in range(group)], axis=0)


def project_kernel(
    count,
    heads,
    tokens,
    gain,
    query_w,
    key_w,
    value_w,
    small_w,
    query_o,
    key_o,
    value_o,
    small_o,
    small_parts,
    small_in,
    small_mid,
    small_mid_in,
    parts,
    arrivals,
    middle,
    middle_in,
    send_sems,
    recv_sems,
):
    met = greet(count, 1)
    token_float = tokens[...].astype(F32)
    normed = (token_float * gain[...]).astype(jnp.bfloat16)
    small = jnp.dot(normed, small_w[...], preferred_element_type=F32)
    squares = jnp.sum(token_float * token_float, axis=1, keepdims=True)
    lane = lax.broadcasted_iota(jnp.int32, small.shape, 1)
    put_rows(small_parts, jnp.where(lane == 2 * heads, squares, small), count)
    greeted(met)
    bufs = [(small_parts, small_in, small_mid, small_mid_in)]
    bufs += [tuple(ref.at[p] for ref in (parts, arrivals, middle, middle_in)) for p in range(3)]
    first = [scatter_inner(*bufs[0][:2], send_sems.at[0], recv_sems.at[0], count)]
    for p, weight in enumerate((query_w, key_w, value_w), 1):
        put_rows(bufs[p][0], jnp.dot(normed, weight[...], preferred_element_type=F32), count)
        first.append(scatter_inner(*bufs[p][:2], send_sems.at[p], recv_sems.at[p], count))
    second = [
        scatter_outer(*bufs[p], first[p], send_sems.at[4 + p], recv_sems.at[4 + p], count) for p in range(4)
    ]
    for p, out in enumerate((small_o, query_o, key_o, value_o)):
        out[...] = gathered_sum(bufs[p][2], bufs[p][3], second[p], count)
    for flight in first + second:
        for copy in flight:
            copy.wait_send()


def unit_rows(vectors):
    return vectors * lax.rsqrt(jnp.sum(vectors * vectors, axis=-1, keepdims=True) + epsilon)


def silu(x):
    return x * jax.nn.sigmoid(x)


def softplus(x):
    return jnp.maximum(x, 0.0) + jnp.log(1.0 + jnp.exp(-jnp.abs(x)))


def delta_kernel(
    width,
    query_r,
    key_r,
    value_r,
    small_r,
    rate,
    lengths,
    betas,
    decays,
    keys,
    values,
    state,
    out,
    keys32,
    values32,
    rows_scr,
    held,
    held_sem,
):
    fetch = pltpu.make_async_copy(state, held, held_sem)
    fetch.start()
    rows, heads, head_dim = state.shape[0], state.shape[1], state.shape[2]
    span = betas.shape[2]

    def stack(pieces):
        return jnp.concatenate(pieces, axis=0)

    keys32[...] = keys[...].astype(F32)
    values32[...] = values[...].astype(F32)
    small = small_r[...]
    scale = lax.rsqrt(small[:, 2 * heads : 2 * heads + 1] / width + epsilon)
    scaled = small * scale

    def by_heads(ref):
        raw = ref[...] * scale
        return stack([raw[:, h * head_dim : (h + 1) * head_dim] for h in range(heads)])

    queries = unit_rows(silu(by_heads(query_r)))
    new_key = unit_rows(silu(by_heads(key_r)))
    new_value = silu(by_heads(value_r))
    new_beta = stack([jax.nn.sigmoid(scaled[:, h : h + 1]) for h in range(heads)])
    new_decay = stack(
        [-rate[0, h] * softplus(scaled[:, heads + h : heads + h + 1]) for h in range(heads)]
    )
    live = lax.broadcasted_iota(jnp.int32, (rows, span), 1) < lengths[...]
    beta_live = stack([jnp.where(live, betas[:, h, :], 0.0) for h in range(heads)])
    shrink = stack([jnp.exp(jnp.where(live, decays[:, h, :], 0.0)) for h in range(heads)])

    meet = new_beta * jnp.sum(new_key * queries, axis=1, keepdims=True)
    fade = jnp.exp(new_decay)
    probe = (queries - meet * new_key) * fade
    read = meet * new_value
    for t in range(span - 1, -1, -1):
        k = stack([keys32[pl.ds(h * span + t, rows, stride=heads * span), :] for h in range(heads)])
        v = stack([values32[pl.ds(h * span + t, rows, stride=heads * span), :] for h in range(heads)])
        inverse = lax.rsqrt(jnp.sum(k * k, axis=1, keepdims=True) + epsilon)
        unit = k * inverse
        hit = beta_live[:, t : t + 1] * jnp.sum(unit * probe, axis=1, keepdims=True)
        read = read + hit * v
        probe = shrink[:, t : t + 1] * (probe - hit * unit)
    total = rows * heads
    if total < head_dim:
        probe = jnp.concatenate([probe, jnp.zeros((head_dim - total, head_dim), F32)], axis=0)
    columns = probe.T
    fetch.wait()
    for h in range(heads):
        for r in range(rows):
            n = h * rows + r
            rows_scr[n : n + 1, :] = jnp.sum(columns[:, n : n + 1] * held[r, h], axis=0, keepdims=True)
    final = read + rows_scr[...]
    for h in range(heads):
        out[:, h * head_dim : (h + 1) * head_dim] = final[h * rows : (h + 1) * rows].astype(jnp.bfloat16)


def across_heads(block, mine, arrivals, send_sems, recv_sems, count):
    mine[...] = block
    copies = []
    for offset in range(1, count):
        peer = peer_of("tp", offset, count)
        copies.append(send(mine, arrivals.at[offset], send_sems.at[offset], recv_sems.at[offset], "tp", peer))
    total = block
    for offset in range(1, count):
        copies[offset - 1].wait_recv()
        total = total + arrivals[offset]
    return total, copies


def mixer_kernel(
    count,
    tp_count,
    width,
    head_out,
    tokens,
    gain,
    out_w,
    up_w,
    down_w,
    result,
    heads_all,
    share,
    share_in,
    down_share,
    down_in,
    square_parts,
    square_in,
    square_mid,
    square_mid_in,
    parts,
    arrivals,
    middle,
    middle_in,
    hidden_all,
    kv_send,
    kv_recv,
    tp_send,
    tp_recv,
):
    pieces, piece = parts.shape[0], parts.shape[4]
    outer, inner = place(count)
    slots = iter(range(kv_send.shape[0]))

    def sems():
        slot = next(slots)
        return kv_send.at[slot], kv_recv.at[slot]

    met = greet(count, tp_count)
    heads_all[inner, outer] = head_out[...]
    greeted(met)
    flights = [gather_outer(heads_all, *sems(), count)]
    flights.append(gather_inner(heads_all, flights[0], *sems(), count))
    for copy in flights[1]:
        copy.wait_recv()
    attended = jnp.dot(all_rows(heads_all), out_w[...], preferred_element_type=F32)
    attended, copies = across_heads(
        in_order(attended, count), share, share_in, tp_send.at[0], tp_recv.at[0], tp_count
    )
    flights.append(copies)
    mixed_in = (tokens[...].astype(F32) + attended).astype(jnp.bfloat16).astype(F32)
    squares = jnp.sum(mixed_in * mixed_in, axis=1, keepdims=True)
    bufs = [tuple(ref.at[p] for ref in (parts, arrivals, middle, middle_in)) for p in range(pieces)]
    bufs.append((square_parts, square_in, square_mid, square_mid_in))
    put_rows(square_parts, jnp.broadcast_to(squares, (squares.shape[0], 128)), count)
    square_first = scatter_inner(square_parts, square_in, *sems(), count)
    normed = (mixed_in * gain[...]).astype(jnp.bfloat16)
    first = []
    for p in range(pieces):
        block = jnp.dot(normed, up_w[:, p * piece : (p + 1) * piece], preferred_element_type=F32)
        put_rows(bufs[p][0], block, count)
        first.append(scatter_inner(*bufs[p][:2], *sems(), count))
    square_second = scatter_outer(*bufs[pieces], square_first, *sems(), count)
    second = [scatter_outer(*bufs[p], first[p], *sems(), count) for p in range(pieces)]
    own_squares = gathered_sum(square_mid, square_mid_in, square_second, count)
    scale = lax.rsqrt(own_squares[:, :1] / width + epsilon)
    third = []
    for p in range(pieces):
        raw = gathered_sum(bufs[p][2], bufs[p][3], second[p], count) * scale
        hidden_all[p, inner, outer] = jnp.square(jnp.maximum(raw, 0.0)).astype(jnp.bfloat16)
        third.append(gather_outer(hidden_all.at[p], *sems(), count))
    fourth = [gather_inner(hidden_all.at[p], third[p], *sems(), count) for p in range(pieces)]
    down = jnp.zeros(share.shape, F32)
    for p in range(pieces):
        for copy in fourth[p]:
            copy.wait_recv()
        down = down + jnp.dot(
            all_rows(hidden_all.at[p]),
            down_w[p * piece : (p + 1) * piece, :],
            preferred_element_type=F32,
        )
    down, copies = across_heads(
        in_order(down, count), down_share, down_in, tp_send.at[1], tp_recv.at[1], tp_count
    )
    flights.append(copies)
    result[...] = (mixed_in + down).astype(jnp.bfloat16)
    for flight in flights + [square_first, square_second] + first + second + third + fourth:
        for copy in flight:
            copy.wait_send()


def vmem(count):
    return [pl.BlockSpec(memory_space=pltpu.VMEM)] * count


def local(
    kv,
    tp,
    tokens,
    mix_gain,
    query_weight,
    key_weight,
    value_weight,
    beta_weight,
    decay_weight,
    decay_rate,
    prior_state,
    tail_keys,
    tail_values,
    tail_beta,
    tail_decay,
    lengths,
    out_weight,
    mlp_gain,
    up_weight,
    down_weight,
):
    rows, heads, head_dim = prior_state.shape[:3]
    span = tail_keys.shape[2]
    batch = rows * kv
    depth = mix_gain.shape[0]
    width = depth * kv
    inner = heads * head_dim
    units = up_weight.shape[1]
    piece = min(units, 1024)
    pieces = units // piece
    dma = pltpu.SemaphoreType.DMA
    group = group_of(kv)

    def scatter_buffers(lead, columns, dtype):
        full = pltpu.VMEM(lead + (group, kv // group, rows, columns), dtype)
        middle = pltpu.VMEM(lead + (kv // group, rows, columns), dtype)
        return full, full, middle, middle

    token_rows = lax.all_gather(tokens, "tp", axis=1, tiled=True)
    small_weight = jnp.concatenate(
        [beta_weight, decay_weight, jnp.zeros((depth, 128 - 2 * heads), jnp.bfloat16)], axis=1
    )
    query_s, key_s, value_s, small_s = pl.pallas_call(
        functools.partial(project_kernel, kv, heads),
        out_shape=[jax.ShapeDtypeStruct((rows, inner), F32)] * 3 + [jax.ShapeDtypeStruct((rows, 128), F32)],
        in_specs=vmem(6),
        out_specs=vmem(4),
        scratch_shapes=[
            *scatter_buffers((), 128, F32),
            *scatter_buffers((3,), inner, LINK),
            dma((8, kv)),
            dma((8, kv)),
        ],
        compiler_params=pltpu.CompilerParams(
            collective_id=0, has_side_effects=True, vmem_limit_bytes=12 * 2**20
        ),
        cost_estimate=pl.CostEstimate(flops=2 * 10**10, bytes_accessed=0, transcendentals=0),
        name="project",
    )(token_rows, mix_gain.reshape(1, depth), query_weight, key_weight, value_weight, small_weight)
    count = rows * heads * span
    head_out = pl.pallas_call(
        functools.partial(delta_kernel, width),
        out_shape=jax.ShapeDtypeStruct((rows, inner), jnp.bfloat16),
        in_specs=vmem(4) + [pl.BlockSpec(memory_space=pltpu.SMEM)]
        + vmem(5)
        + [pl.BlockSpec(memory_space=pl.ANY)],
        out_specs=vmem(1)[0],
        scratch_shapes=[
            pltpu.VMEM((count, head_dim), F32),
            pltpu.VMEM((count, head_dim), F32),
            pltpu.VMEM((rows * heads, head_dim), F32),
            pltpu.VMEM(prior_state.shape, F32),
            pltpu.SemaphoreType.DMA,
        ],
        compiler_params=pltpu.CompilerParams(vmem_limit_bytes=57 * 2**20),
        name="delta",
    )(
        query_s,
        key_s,
        value_s,
        small_s,
        decay_rate.reshape(1, heads),
        lengths.reshape(rows, 1),
        tail_beta,
        tail_decay,
        tail_keys.reshape(count, head_dim),
        tail_values.reshape(count, head_dim),
        prior_state,
    )
    slots = 4 + 4 * pieces
    result = pl.pallas_call(
        functools.partial(mixer_kernel, kv, tp, width),
        out_shape=jax.ShapeDtypeStruct((batch, depth), jnp.bfloat16),
        in_specs=vmem(6),
        out_specs=vmem(1)[0],
        scratch_shapes=[
            pltpu.VMEM((group, kv // group, rows, inner), jnp.bfloat16),
            pltpu.VMEM((batch, depth), F32),
            pltpu.VMEM((tp, batch, depth), F32),
            pltpu.VMEM((batch, depth), F32),
            pltpu.VMEM((tp, batch, depth), F32),
            *scatter_buffers((), 128, F32),
            *scatter_buffers((pieces,), piece, LINK),
            pltpu.VMEM((pieces, group, kv // group, rows, piece), jnp.bfloat16),
            dma((slots, kv)),
            dma((slots, kv)),
            dma((2, tp)),
            dma((2, tp)),
        ],
        compiler_params=pltpu.CompilerParams(
            collective_id=1, has_side_effects=True, vmem_limit_bytes=20 * 2**20
        ),
        name="mixer",
    )(head_out, token_rows, mlp_gain.reshape(1, depth), out_weight, up_weight, down_weight)
    columns = depth // tp
    return lax.dynamic_slice_in_dim(result, lax.axis_index("tp") * columns, columns, axis=1)


def solution(mesh):
    in_specs = (
        P(None, ("kv", "tp")),
        P("kv"),
        P("kv", "tp"),
        P("kv", "tp"),
        P("kv", "tp"),
        P("kv", "tp"),
        P("kv", "tp"),
        P("tp"),
        P("kv", "tp", None, None),
        P("kv", "tp", None, None),
        P("kv", "tp", None, None),
        P("kv", "tp", None),
        P("kv", "tp", None),
        P("kv"),
        P("tp", "kv"),
        P("kv"),
        P("kv", "tp"),
        P("tp", "kv"),
    )
    out_specs = P(None, ("kv", "tp"))
    body = functools.partial(local, mesh.shape["kv"], mesh.shape["tp"])
    return jax.shard_map(body, mesh=mesh, in_specs=in_specs, out_specs=out_specs, check_vma=False)
```

time: 120 us -> 99.6 us (0.83)
  Pallas kernels: 104 us -> 87 us
  local copies, waits for them, and re-layouts: 13.6 us -> 9.89 us
    pallas_call x1, Pallas kernels: 64.7 us -> 50.6 us  [local(): pl.pallas_call(functools.partial(mixer_kernel, kv, tp, width), out_shape=...]
    unnamed x30, local copies, waits for them, and re-layouts: 11.9 us -> 8.25 us
    pallas_call x1, Pallas kernels: 25.4 us -> 21.9 us  [local(): pl.pallas_call(functools.partial(project_kernel, kv, heads), out_shape=[j...]
where the time goes in v2:
time: 99.6 us; the launch traced here: 99.2 us
  Pallas kernels  87 us (87%)
  local copies, waits for them, and re-layouts  9.89 us (10%)
  blocking collectives  2.17 us (2%)
    pallas_call x1, Pallas kernels, local(): pl.pallas_call(functools.partial(mixer_kernel, kv, tp, width), out_shape=...  50.6 us
    pallas_call x1, Pallas kernels, local(): pl.pallas_call(functools.partial(project_kernel, kv, heads), out_shape=[j...  21.9 us
    pallas_call x1, Pallas kernels, local(): pl.pallas_call(functools.partial(delta_kernel, width), out_shape=jax.Shap...  14.5 us
    unnamed x30, local copies, waits for them, and re-layouts  8.25 us
    all_gather x1, blocking collectives, local(): token_rows = lax.all_gather(tokens, 'tp', axis=1, tiled=True)  2.17 us

profile of v2, /device:TPU:0, one launch (start us, length us, event | category | flops | bytes accessed | tf_op | source)
XLA Modules:
  0.0 99.2 jit_solution(4667967596806005131)
XLA Ops:
  0.0 2.2 %all_gather.3 = bf16[128,128]{0,1:T(8,128)(2,1)S(1)} all-gather(bf16[128,64]{0,1:T(8,128)(2,1)} %param.18), channel_id=1, replica_groups=mesh['kv'=16,'tp'=2] {'tp'}, dimensions={1}, use_global_device_ids=true | all-gather | bytes 49152 | tf_op jit(solution)/shard_map/all_gather | solution.py:440
  2.2 0.1 copy.26.tokens
  2.3 0.8 copy.24
  3.1 0.8 copy.25
  3.9 0.1 pad.2.clone
  4.0 0.1 maximum_maximum_fusion.small_w
  4.1 0.0 copy-start.9
  4.1 0.9 copy-done.9
  5.0 0.9 copy-done.10
  6.0 0.9 copy-done.11
  6.9 0.7 copy-done.12
  7.6 21.9 %project.1 = (f32[8,1024]{1,0:T(8,128)S(1)}, f32[8,1024]{1,0:T(8,128)S(1)}, f32[8,1024]{1,0:T(8,128)S(1)}, f32[8,128]{1,0:T(8,128)S(1)}) custom-call(bf16[128,128]{1,0:T(8,128)(2,1)S(1)} %copy.26.tokens, f32[1,128]{1,0:T(1,128)S(1)} %bitcast.7, bf16[128,1024]{1,0:T(8,128)(2,1)S(1)} %copy-done.9, bf16[128,1024]{1,0:T(8,128)(2,1)S(1)} %copy-done.10, ...), custom_call_target="tpu_custom_call" | custom-call | flops 20000000000 | tf_op jit(solution)/shard_map/project/pallas_call | solution.py:444
  29.5 0.6 copy-done.4
  30.1 0.6 copy-done.5
  30.7 0.6 copy-done.6
  31.3 0.6 copy-done.7
  31.9 0.0 copy-done.13
  31.9 0.7 copy.27.lengths
  32.6 14.5 %delta.1.head_out = bf16[8,1024]{1,0:T(8,128)(2,1)} custom-call(f32[8,1024]{1,0:T(8,128)} %copy-done.4, f32[8,1024]{1,0:T(8,128)} %copy-done.5, f32[8,1024]{1,0:T(8,128)} %copy-done.6, f32[8,128]{1,0:T(8,128)} %copy-done.7, f32[1,8]{1,0:T(1,128)} %bitcast.10, s32[8,1]{1,0:T(8,128)} %copy.27.lengths, f32[8,8,64]{2,1,0:T(8,128)} %betas.1, f32[8,8,64]{2,1,0:T(8,128)} %decays.1, ...), custom_call_target="tpu_custom_call" | custom-call | tf_op jit(solution)/shard_map/delta/pallas_call | solution.py:462
  47.1 0.0 copy-start.3
  47.1 0.7 copy-done.3
  47.8 50.6 %mixer.1 = bf16[128,128]{1,0:T(8,128)(2,1)S(1)} custom-call(bf16[8,1024]{1,0:T(8,128)(2,1)S(1)} %copy-done.3, bf16[128,128]{1,0:T(8,128)(2,1)S(1)} %copy.26.tokens, f32[1,128]{1,0:T(1,128)S(1)} %bitcast.6, bf16[1024,128]{1,0:T(8,128)(2,1)S(1)} %copy-done.2, bf16[128,4096]{1,0:T(8,128)(2,1)S(1)} %copy-done, bf16[4096,128]{1,0:T(8,128)(2,1)S(1)} %copy-done.1), custom_call_target="tpu_custom_call" | custom-call | tf_op jit(solution)/shard_map/mixer/pallas_call | solution.py:492
  98.4 0.1 constant_dynamic-slice_fusion
  98.5 0.7 copy.29
  (17 shorter events, 0.0 us)
Async XLA Ops:
  4.1 1.0 copy-start.9
  5.0 0.9 copy-start.10
  6.0 0.9 copy-start.11
  6.9 0.7 copy-start.12
  7.6 24.3 %copy-start.13 = (s32[8]{0:T(128)S(1)}, s32[8]{0:T(128)}, u32[]{:S(2)}) copy-start(s32[8]{0:T(128)} %param.31) | copy-start | bytes 100
  29.5 0.6 copy-start.4
  30.1 0.6 copy-start.5
  30.7 0.6 copy-start.6
  31.3 0.6 copy-start.7
  31.9 15.2 %copy-start = (bf16[128,4096]{1,0:T(8,128)(2,1)S(1)}, bf16[128,4096]{1,0:T(8,128)(2,1)}, u32[]{:S(2)}) copy-start(bf16[128,4096]{1,0:T(8,128)(2,1)} %up_w.1) | copy-start | bytes 3145732
  31.9 15.2 %copy-start.1 = (bf16[4096,128]{1,0:T(8,128)(2,1)S(1)}, bf16[4096,128]{1,0:T(8,128)(2,1)}, u32[]{:S(2)}) copy-start(bf16[4096,128]{1,0:T(8,128)(2,1)} %down_w.1) | copy-start | bytes 3145732
  31.9 15.2 %copy-start.2 = (bf16[1024,128]{1,0:T(8,128)(2,1)S(1)}, bf16[1024,128]{1,0:T(8,128)(2,1)}, u32[]{:S(2)}) copy-start(bf16[1024,128]{1,0:T(8,128)(2,1)} %out_w.1) | copy-start | bytes 786436
  31.9 15.2 %copy-start.8 = (f32[128]{0:T(128)S(1)}, f32[128]{0:T(128)}, u32[]{:S(2)}) copy-start(f32[128]{0:T(128)} %param.33) | copy-start | bytes 1540
  47.1 0.7 copy-start.3

commit v3 on v2

--- a/solution.py
+++ b/solution.py
@@ -453,7 +453,7 @@
             dma((8, kv)),
         ],
         compiler_params=pltpu.CompilerParams(
-            collective_id=0, has_side_effects=True, vmem_limit_bytes=12 * 2**20
+            collective_id=0, has_side_effects=True, vmem_limit_bytes=57 * 2**20
         ),
         cost_estimate=pl.CostEstimate(flops=2 * 10**10, bytes_accessed=0, transcendentals=0),
         name="project",

time: 99.6 us -> 96.6 us (0.970)
  local copies, waits for them, and re-layouts: 9.89 us -> 4.58 us
  Pallas kernels: 87 us -> 88.7 us
    unnamed x30 -> x16, local copies, waits for them, and re-layouts: 8.25 us -> 2.34 us
    pallas_call x1, Pallas kernels: 21.9 us -> 23.7 us  [local(): pl.pallas_call(functools.partial(project_kernel, kv, heads), out_shape=[j...]
where the time goes in v3:
time: 96.6 us; the launch traced here: 96.3 us
  Pallas kernels  88.7 us (92%)
  local copies, waits for them, and re-layouts  4.58 us (5%)
  blocking collectives  2.17 us (2%)
    pallas_call x1, Pallas kernels, local(): pl.pallas_call(functools.partial(mixer_kernel, kv, tp, width), out_shape=...  50.6 us
    pallas_call x1, Pallas kernels, local(): pl.pallas_call(functools.partial(project_kernel, kv, heads), out_shape=[j...  23.7 us
    pallas_call x1, Pallas kernels, local(): pl.pallas_call(functools.partial(delta_kernel, width), out_shape=jax.Shap...  14.5 us
    unnamed x16, local copies, waits for them, and re-layouts  2.34 us
    all_gather x1, blocking collectives, local(): token_rows = lax.all_gather(tokens, 'tp', axis=1, tiled=True)  2.17 us

profile of v3, /device:TPU:0, one launch (start us, length us, event | category | flops | bytes accessed | tf_op | source)
XLA Modules:
  0.0 96.3 jit_solution(10454530587547488582)
XLA Ops:
  0.0 2.2 %all_gather.3 = bf16[128,128]{0,1:T(8,128)(2,1)S(1)} all-gather(bf16[128,64]{0,1:T(8,128)(2,1)} %param.18), channel_id=1, replica_groups=mesh['kv'=16,'tp'=2] {'tp'}, dimensions={1}, use_global_device_ids=true | all-gather | bytes 49152 | tf_op jit(solution)/shard_map/all_gather | solution.py:440
  2.2 0.7 copy.26.tokens
  2.9 0.8 copy.24
  3.7 0.8 copy.25
  4.5 0.1 pad.2.clone
  4.6 0.7 maximum_maximum_fusion.small_w
  5.2 23.7 %project.1 = (f32[8,1024]{1,0:T(8,128)}, f32[8,1024]{1,0:T(8,128)}, f32[8,1024]{1,0:T(8,128)}, f32[8,128]{1,0:T(8,128)}) custom-call(bf16[128,128]{1,0:T(8,128)(2,1)} %copy.26.tokens, f32[1,128]{1,0:T(1,128)} %bitcast.11, bf16[128,1024]{1,0:T(8,128)(2,1)} %query_w.1, bf16[128,1024]{1,0:T(8,128)(2,1)} %key_w.1, bf16[128,1024]{1,0:T(8,128)(2,1)} %value_w.1, ...), custom_call_target="tpu_custom_call" | custom-call | flops 20000000000 | tf_op jit(solution)/shard_map/project/pallas_call | solution.py:444
  28.9 0.0 copy-start
  28.9 0.0 copy-start.1
  28.9 0.0 copy-start.2
  29.0 0.0 copy-start.3
  29.0 0.0 copy-start.5
  29.0 0.7 copy.27.lengths
  29.7 14.5 %delta.1.head_out = bf16[8,1024]{1,0:T(8,128)(2,1)} custom-call(f32[8,1024]{1,0:T(8,128)} %get-tuple-element.9.query_r, f32[8,1024]{1,0:T(8,128)} %get-tuple-element.10.key_r, f32[8,1024]{1,0:T(8,128)} %get-tuple-element.11.value_r, f32[8,128]{1,0:T(8,128)} %get-tuple-element.12.small_r, f32[1,8]{1,0:T(1,128)} %bitcast.9, s32[8,1]{1,0:T(8,128)} %copy.27.lengths, ...), custom_call_target="tpu_custom_call" | custom-call | tf_op jit(solution)/shard_map/delta/pallas_call | solution.py:462
  44.1 0.0 copy-done
  44.1 0.0 copy-done.1
  44.1 0.0 copy-done.2
  44.2 0.0 copy-done.3
  44.2 0.0 copy-done.5
  44.2 0.0 copy-start.4
  44.2 0.7 copy-done.4
  44.9 50.6 %mixer.1 = bf16[128,128]{1,0:T(8,128)(2,1)S(1)} custom-call(bf16[8,1024]{1,0:T(8,128)(2,1)S(1)} %copy-done.4, bf16[128,128]{1,0:T(8,128)(2,1)S(1)} %copy-done.3, f32[1,128]{1,0:T(1,128)S(1)} %bitcast.6, bf16[1024,128]{1,0:T(8,128)(2,1)S(1)} %copy-done.2, bf16[128,4096]{1,0:T(8,128)(2,1)S(1)} %copy-done, bf16[4096,128]{1,0:T(8,128)(2,1)S(1)} %copy-done.1), custom_call_target="tpu_custom_call" | custom-call | tf_op jit(solution)/shard_map/mixer/pallas_call | solution.py:492
  95.5 0.1 constant_dynamic-slice_fusion
  95.6 0.7 copy.29
  (3 shorter events, 0.0 us)
Async XLA Ops:
  5.2 23.7 %copy-start.6 = (s32[8]{0:T(128)S(1)}, s32[8]{0:T(128)}, u32[]{:S(2)}) copy-start(s32[8]{0:T(128)} %param.31) | copy-start | bytes 100
  28.9 15.2 %copy-start = (bf16[128,4096]{1,0:T(8,128)(2,1)S(1)}, bf16[128,4096]{1,0:T(8,128)(2,1)}, u32[]{:S(2)}) copy-start(bf16[128,4096]{1,0:T(8,128)(2,1)} %up_w.1) | copy-start | bytes 3145732
  28.9 15.2 %copy-start.1 = (bf16[4096,128]{1,0:T(8,128)(2,1)S(1)}, bf16[4096,128]{1,0:T(8,128)(2,1)}, u32[]{:S(2)}) copy-start(bf16[4096,128]{1,0:T(8,128)(2,1)} %down_w.1) | copy-start | bytes 3145732
  28.9 15.2 %copy-start.2 = (bf16[1024,128]{1,0:T(8,128)(2,1)S(1)}, bf16[1024,128]{1,0:T(8,128)(2,1)}, u32[]{:S(2)}) copy-start(bf16[1024,128]{1,0:T(8,128)(2,1)} %out_w.1) | copy-start | bytes 786436
  29.0 15.2 %copy-start.3 = (bf16[128,128]{1,0:T(8,128)(2,1)S(1)}, bf16[128,128]{1,0:T(8,128)(2,1)}, u32[]{:S(2)}) copy-start(bf16[128,128]{1,0:T(8,128)(2,1)} %copy.26.tokens) | copy-start | bytes 98308
  29.0 15.2 %copy-start.5 = (f32[128]{0:T(128)S(1)}, f32[128]{0:T(128)}, u32[]{:S(2)}) copy-start(f32[128]{0:T(128)} %param.33) | copy-start | bytes 1540
  44.2 0.7 copy-start.4
